TPU v7x, 128 devices: a whole 4x4x4 slice. The times are simulated.
128 devices in a mesh: sp: 16 (over z, y), tp: 8 (over x, core).
Axes of the slice: x: 4, y: 4, z: 4, core: 2. Of those that a mesh axis runs over, the one named last changes fastest.
Arguments:
- layer_input: bfloat16 [16, 4096, 2048], P(None, ('sp', 'tp')), may hold values from -6 to 6
- input_gain: float32 [2048], replicated, may hold values from 0.5 to 1.5
- narrowing_matrix: bfloat16 [2048, 512], replicated, may hold values from -0.125 to 0.125
- rotary_down: bfloat16 [2048, 64], replicated, may hold values from -0.125 to 0.125
- summary_scaling: float32 [512], replicated, may hold values from 0.5 to 1.5
- lookup_widening: bfloat16 [512, 16, 128], P('tp'), may hold values from -0.25 to 0.25
- payload_widening: bfloat16 [512, 16, 128], P('tp'), may hold values from -0.25 to 0.25
- query_nope: bfloat16 [16, 16, 128], P('sp', 'tp'), may hold values from -6 to 6
- query_rotary: bfloat16 [16, 16, 64], P('sp', 'tp'), may hold values from -6 to 6
Outputs:
- stored_summaries: bfloat16 [16, 4096, 512], P('sp', None, 'tp')
- rotary_cache: bfloat16 [16, 4096, 64], P('sp', None, 'tp')
- first_read: bfloat16 [16, 16, 128], P('sp', 'tp')
All inputs are finite; a program needn't handle non-finite values.
Results may differ from a plain program's by a relative error of at most 0.02.
Values may be sent and summed in bfloat16 or wider, within the bound.
A program may use at most 64 MiB of HBM per device.

v0:
```python
import jax
import jax.numpy as jnp
from jax import lax
from jax.sharding import Mesh
from jax.sharding import PartitionSpec as P

QK_ROPE = 64
PLAIN_MATCH_SPAN = 128
TP = ("tp_0", "tp_1")
SP_TP = ("sp", "tp_0", "tp_1")
norm_eps = 1e-06
rotary_base = 10000.0


def joined_along(parts, dim):
    parts = jnp.moveaxis(parts, 0, dim)
    lengths = parts.shape
    return parts.reshape(*lengths[:dim], lengths[dim] * lengths[dim + 1], *lengths[dim + 2 :])


def gather_together(arrays, axis, dims):
    line = jnp.concatenate([a.reshape(-1) for a in arrays])
    lines, at, finished = (lax.all_gather(line, axis), 0, [])
    for a, dim in zip(arrays, dims):
        parts = lines[:, at : at + a.size].reshape(-1, *a.shape)
        finished.append(joined_along(parts, dim))
        at += a.size
    return tuple(finished)


def total_of_pieces(array, axis):
    parts = lax.all_gather(array, axis).astype(jnp.float32)
    return parts.sum(axis=0)


def summed_rows(term, width, axes):
    subtotal = term(jnp.int32(0), width * lax.axis_size(axes))
    for axis in axes:
        subtotal = lax.psum_scatter(subtotal, axis, scatter_dimension=0, tiled=True)
    return subtotal


def rescaled_lines(vector):
    return vector * lax.rsqrt(jnp.mean(vector * vector, axis=-1, keepdims=True) + norm_eps)


def rotate(vector, position):
    half_width = vector.shape[-1] // 2
    frequency = 1.0 / rotary_base ** (
        jnp.arange(half_width, dtype=jnp.float32) * 2.0 / vector.shape[-1]
    )
    angles = position * frequency
    first_half = vector[..., :half_width]
    second_half = vector[..., half_width:]
    return jnp.concatenate(
        [
            first_half * jnp.cos(angles) - second_half * jnp.sin(angles),
            second_half * jnp.cos(angles) + first_half * jnp.sin(angles),
        ],
        axis=-1,
    )


def to_pieces(array, sp_count, tp_count):
    seq_count, pos_local, cache_width = array.shape
    seq_each = seq_count // sp_count
    width_each = cache_width // tp_count
    array = array.reshape(sp_count, seq_each, pos_local, tp_count, width_each)
    array = array.transpose(0, 3, 1, 2, 4)
    return array.reshape(sp_count * tp_count, seq_each, pos_local, width_each)


def shards(
    layer_input,
    input_gain,
    narrowing_matrix,
    rotary_down,
    summary_scaling,
    lookup_widening,
    payload_widening,
    query_nope,
    query_rotary,
):
    seq_count, pos_local, feature_width = layer_input.shape
    sp_count = lax.axis_size("sp")
    tp_count = lax.axis_size(TP)
    block_index = lax.axis_index(SP_TP)
    normed = (rescaled_lines(layer_input.astype(jnp.float32)) * input_gain).astype(jnp.bfloat16)
    flat_rows = normed.reshape(seq_count * pos_local, feature_width)
    hidden_summary = jnp.dot(
        flat_rows, narrowing_matrix, preferred_element_type=jnp.float32
    ).astype(jnp.bfloat16)
    rotary = jnp.dot(flat_rows, rotary_down, preferred_element_type=jnp.float32).astype(
        jnp.bfloat16
    )
    hidden_summary = (
        (rescaled_lines(hidden_summary.astype(jnp.float32)) * summary_scaling)
        .astype(jnp.bfloat16)
        .reshape(seq_count, pos_local, -1)
    )
    positions = (block_index * pos_local + jnp.arange(pos_local, dtype=jnp.int32)).astype(
        jnp.float32
    )[None, :, None]
    rotary = rotate(rotary.astype(jnp.float32).reshape(seq_count, pos_local, -1), positions).astype(
        jnp.bfloat16
    )
    moved = (
        lax.all_to_all(
            to_pieces(hidden_summary, sp_count, tp_count),
            SP_TP,
            split_axis=0,
            concat_axis=2,
            tiled=True,
        ),
        lax.all_to_all(
            to_pieces(rotary, sp_count, tp_count), SP_TP, split_axis=0, concat_axis=2, tiled=True
        ),
    )
    hidden_summary = moved[0][0]
    rotary = moved[1][0]
    pos_total = hidden_summary.shape[1]
    rot_each = rotary.shape[2]
    head_each = query_nope.shape[1]
    query_all, turn_all = gather_together((query_nope, query_rotary), TP, (1, 1))
    absorbed = jnp.einsum(
        "shd,chd->shc", query_all, lookup_widening, preferred_element_type=jnp.float32
    ).astype(jnp.bfloat16)
    query_turned = rotate(turn_all.astype(jnp.float32), jnp.float32(pos_total)).astype(jnp.bfloat16)
    turned_mine = lax.dynamic_slice_in_dim(query_turned, lax.axis_index(TP) * rot_each, rot_each, 2)
    score_scale = (PLAIN_MATCH_SPAN + QK_ROPE) ** (-0.5)
    partial_value = (
        jnp.einsum("shc,spc->shp", absorbed, hidden_summary, preferred_element_type=jnp.float32)
        + jnp.einsum("shr,spr->shp", turned_mine, rotary, preferred_element_type=jnp.float32)
    ) * score_scale
    scores = total_of_pieces(partial_value.astype(jnp.bfloat16), TP).astype(jnp.float32)
    attention = jax.nn.softmax(scores, axis=-1).astype(jnp.bfloat16)
    context = jnp.einsum(
        "shp,spc->shc", attention, hidden_summary, preferred_element_type=jnp.float32
    ).astype(jnp.bfloat16)

    def project_heads(row_start, row_count):
        part_context = lax.dynamic_slice_in_dim(context, row_start, row_count, 1)
        part_weight = lax.dynamic_slice_in_dim(payload_widening, row_start, row_count, 1)
        return jnp.einsum(
            "shc,chv->hsv", part_context, part_weight, preferred_element_type=jnp.float32
        )

    values = summed_rows(project_heads, head_each, TP)
    first_read = rescaled_lines(values.transpose(1, 0, 2)).astype(jnp.bfloat16)
    return (hidden_summary, rotary, first_read)


def solution(mesh):
    torus = Mesh(mesh.devices.reshape(mesh.shape["sp"], 4, 2), ("sp", "tp_0", "tp_1"))
    in_specs = (
        P(None, SP_TP, None),
        P(),
        P(),
        P(),
        P(),
        P(TP, None, None),
        P(TP, None, None),
        P("sp", TP, None),
        P("sp", TP, None),
    )
    out_specs = (P("sp", None, TP), P("sp", None, TP), P("sp", TP, None))
    return jax.shard_map(
        shards, mesh=torus, in_specs=in_specs, out_specs=out_specs, check_vma=False
    )
```

profile of v0, /device:TPU:1, one launch (start us, length us, event | category | flops | bytes accessed | tf_op | source)
XLA Modules:
  0.0 115.7 jit_solution(14926533977251242927)
XLA Ops:
  7.2 2.2 %fusion.2 = f32[16,32]{1,0:T(8,128)S(1)} fusion(bf16[16,32,2048]{2,1,0:T(8,128)(2,1)} %param.9), kind=kLoop, calls=%fused_computation.5 | loop fusion | flops 3145216 | bytes 2099200 | tf_op jit(solution)/shard_map/reduce_sum | solution.py:44
  9.6 0.5 fusion.4
  10.1 1.3 %copy-done.2 = bf16[16,32,2048]{2,1,0:T(8,128)(2,1)} copy-done((bf16[16,32,2048]{2,1,0:T(8,128)(2,1)}, bf16[16,32,2048]{2,1,0:T(8,128)(2,1)S(1)}, u32[]{:S(2)}) %copy-start.2) | copy-done | bytes 2097176
  11.5 0.8 fusion.5
  13.0 0.8 reshape.408
  13.8 11.5 %all-to-all-start.1 = ((bf16[128,2,128]{2,1,0:T(2,128)(2,1)}), bf16[128,2,128]{2,1,0:T(2,128)(2,1)S(1)}, u32[]{:S(2)}, u32[]{:S(2)}) async-start(bf16[128,2,128]{2,1,0:T(2,128)(2,1)} %reshape.408), calls=%async_computation.1 | async-start | bytes 131072 | tf_op jit(solution)/shard_map/all_to_all | solution.py:115
  25.4 12.3 %all-gather.2 = bf16[8,1,384]{2,1,0:T(2,128)(2,1)S(1)} all-gather(bf16[1,1,384]{2,1,0:T(2,128)(2,1)S(1)} %reshape.390), channel_id=2, replica_groups=mesh['sp'=16,'tp_0'=4,'tp_1'=2] {'tp_0','tp_1'}, dimensions={0}, use_global_device_ids=true | all-gather | bytes 6912 | tf_op jit(solution)/shard_map/all_gather | solution.py:23
  37.7 2.9 %fusion.7 = (f32[512]{0:T(512)S(1)}, bf16[512,512]{0,1:T(8,128)(2,1)S(1)}) fusion(bf16[512,2048]{1,0:T(8,128)(2,1)} %bitcast.76, bf16[2048,512]{1,0:T(8,128)(2,1)S(1)} %copy-done), kind=kOutput, calls=%fused_computation.16 | convolution fusion | flops 1074789888 | bytes 4720640 | tf_op jit(solution)/shard_map/dot_general | solution.py:90
  40.9 1.0 copy.36
  41.9 1.6 %reshape_reshape.3 = bf16[16,1,32,8,64]{4,3,2,0,1:T(8,128)(2,1)S(1)} reshape(bf16[512,512]{1,0:T(8,128)(2,1)} %copy.36) | data formatting | bytes 1048576 | tf_op jit(solution)/shard_map/reshape;reshape | solution.py:68
  43.5 1.2 %copy.37 = bf16[16,8,1,32,64]{4,3,1,0,2:T(8,128)(2,1)} copy(bf16[16,8,1,32,64]{4,1,3,0,2:T(8,128)(2,1)S(1)} %bitcast.77) | data formatting | bytes 1048576 | tf_op jit(solution)/shard_map/transpose | solution.py:69
  44.7 3.0 %reshape.406 = bf16[128,2,1024]{2,1,0:T(2,128)(2,1)} reshape(bf16[128,1,32,64]{3,2,1,0:T(8,128)(2,1)} %bitcast.78) | data formatting | bytes 1048576
  47.8 8.9 %all-to-all-start = ((bf16[128,2,1024]{2,1,0:T(2,128)(2,1)}), bf16[128,2,1024]{2,1,0:T(2,128)(2,1)}, u32[]{:S(2)}, u32[]{:S(2)}) async-start(bf16[128,2,1024]{2,1,0:T(2,128)(2,1)} %reshape.406), calls=%async_computation | async-start | bytes 1048576 | tf_op jit(solution)/shard_map/all_to_all | solution.py:108
  56.9 0.2 fusion.15
  57.1 0.2 reshape.409
  57.4 0.3 reshape.382
  57.6 12.3 %all-to-all-done = bf16[128,2,1024]{2,1,0:T(2,128)(2,1)} async-done(((bf16[128,2,1024]{2,1,0:T(2,128)(2,1)}), bf16[128,2,1024]{2,1,0:T(2,128)(2,1)}, u32[]{:S(2)}, u32[]{:S(2)}) %all-to-all-start) | async-done | bytes 524320 | tf_op jit(solution)/shard_map/all_to_all | solution.py:108
  69.9 2.3 %reshape.407 = bf16[128,1,32,64]{3,2,1,0:T(8,128)(2,1)S(1)} reshape(bf16[128,2,1024]{2,1,0:T(2,128)(2,1)} %all-to-all-done) | data formatting | bytes 1048576
  72.2 0.4 fusion.26
  72.6 0.9 fusion.1
  73.5 0.6 dynamic-slice.2
  74.1 0.6 dynamic-slice
  76.0 0.9 squeeze.7
  76.9 1.1 copy.45
  78.0 15.5 %all-gather.5.cloned.1.call-done = bf16[128,4096]{1,0:T(8,128)(2,1)} async-done(((bf16[16,4096]{1,0:T(8,128)(2,1)}), bf16[128,4096]{1,0:T(8,128)(2,1)}) %all-gather.5.cloned.1.call-update) | async-done | bytes 1048592 | tf_op jit(solution)/shard_map/all_gather | solution.py:32
  93.6 1.4 %convert_reduce_fusion = f32[16,4096]{1,0:T(8,128)S(1)} fusion(bf16[8,16,4096]{2,1,0:T(8,128)(2,1)} %bitcast.80), kind=kLoop, calls=%fused_computation.8 | loop fusion | flops 983040 | bytes 1310720 | tf_op jit(solution)/shard_map/reduce_sum | solution.py:33
  95.1 0.2 exponential_reduce_fusion
  95.3 0.3 fusion.6
  95.7 1.1 fusion.13
  96.8 6.9 %all-reduce = f32[16,1,128]{2,0,1:T(8,128)S(1)} all-reduce(f32[16,1,128]{2,0,1:T(8,128)S(1)} %bitcast.86), channel_id=4, replica_groups=mesh['sp'=16,'tp_0'=4,'tp_1'=2] {'tp_0'}, use_global_device_ids=true, to_apply=%region_5.0.clone | all-reduce | flops 2048 | bytes 16384
  103.7 4.4 %all-reduce.1 = f32[4,1,128]{2,0,1:T(4,128)S(1)} all-reduce(f32[4,1,128]{2,0,1:T(4,128)S(1)} %constant_dynamic-slice_fusion), channel_id=5, replica_groups=mesh['sp'=16,'tp_0'=4,'tp_1'=2] {'tp_1'}, use_global_device_ids=true, to_apply=%region_6.0.clone | all-reduce | flops 512 | bytes 4096
  108.3 0.6 multiply_convert_fusion
  (49 shorter events, 1.7 us)
Async XLA Ops:
  7.2 30.5 %copy-start = (bf16[2048,512]{1,0:T(8,128)(2,1)S(1)}, bf16[2048,512]{1,0:T(8,128)(2,1)}, u32[]{:S(2)}) copy-start(bf16[2048,512]{1,0:T(8,128)(2,1)} %param.11) | copy-start | bytes 6291460
  7.2 2.3 %copy-start.4 = (f32[2048]{0:T(1024)S(1)}, f32[2048]{0:T(1024)}, u32[]{:S(2)}) copy-start(f32[2048]{0:T(1024)} %param.10) | copy-start | bytes 24580
  7.2 2.3 %copy-start.1 = (bf16[16,32,2048]{2,1,0:T(8,128)(2,1)S(1)}, bf16[16,32,2048]{2,1,0:T(8,128)(2,1)}, u32[]{:S(2)}) copy-start(bf16[16,32,2048]{2,1,0:T(8,128)(2,1)} %param.9) | copy-start | bytes 6291460
  9.6 1.9 %copy-start.3 = (bf16[2048,64]{0,1:T(8,128)(2,1)S(1)}, bf16[2048,64]{0,1:T(8,128)(2,1)}, u32[]{:S(2)}) copy-start(bf16[2048,64]{0,1:T(8,128)(2,1)} %param.12) | copy-start | bytes 786436
  10.1 1.4 %copy-start.2 = (bf16[16,32,2048]{2,1,0:T(8,128)(2,1)}, bf16[16,32,2048]{2,1,0:T(8,128)(2,1)S(1)}, u32[]{:S(2)}) copy-start(bf16[16,32,2048]{2,1,0:T(8,128)(2,1)S(1)} %fusion.4) | copy-start | bytes 6291460
  11.5 13.8 %copy-start.8 = (bf16[1,2,64]{2,1,0:T(2,128)(2,1)S(1)}, bf16[1,2,64]{2,1,0:T(2,128)(2,1)}, u32[]{:S(2)}) copy-start(bf16[1,2,64]{2,1,0:T(2,128)(2,1)} %param.17) | copy-start | bytes 772
  11.5 13.9 %copy-start.6 = (bf16[1,2,128]{2,1,0:T(2,128)(2,1)S(1)}, bf16[1,2,128]{2,1,0:T(2,128)(2,1)}, u32[]{:S(2)}) copy-start(bf16[1,2,128]{2,1,0:T(2,128)(2,1)} %param.16) | copy-start | bytes 1540
  13.8 34.0 %all-to-all-start.1 = ((bf16[128,2,128]{2,1,0:T(2,128)(2,1)}), bf16[128,2,128]{2,1,0:T(2,128)(2,1)S(1)}, u32[]{:S(2)}, u32[]{:S(2)}) async-start(bf16[128,2,128]{2,1,0:T(2,128)(2,1)} %reshape.408), calls=%async_computation.1 | async-start | bytes 131072 | tf_op jit(solution)/shard_map/all_to_all | solution.py:115
  37.6 2.9 %copy-start.5 = (f32[512]{0:T(512)S(1)}, f32[512]{0:T(512)}, u32[]{:S(2)}) copy-start(f32[512]{0:T(512)} %param.13) | copy-start | bytes 6148
  44.7 12.1 %copy-start.7 = (bf16[64,16,128]{2,1,0:T(8,128)(2,1)S(1)}, bf16[64,16,128]{2,1,0:T(8,128)(2,1)}, u32[]{:S(2)}) copy-start(bf16[64,16,128]{2,1,0:T(8,128)(2,1)} %param.14) | copy-start | bytes 786436
  47.8 22.2 %all-to-all-start = ((bf16[128,2,1024]{2,1,0:T(2,128)(2,1)}), bf16[128,2,1024]{2,1,0:T(2,128)(2,1)}, u32[]{:S(2)}, u32[]{:S(2)}) async-start(bf16[128,2,1024]{2,1,0:T(2,128)(2,1)} %reshape.406), calls=%async_computation | async-start | bytes 1048576 | tf_op jit(solution)/shard_map/all_to_all | solution.py:108
  56.7 36.9 %all-gather.5.cloned.1.call-start = ((), (), s32[]{:S(2)}) async-start(), calls=%async_computation.2 | async-start | bytes 1179648 | tf_op jit(solution)/shard_map/all_gather | solution.py:32
  57.3 16.2 %copy-start.10 = (u32[128]{0:T(128)S(1)}, u32[128]{0:T(128)}, u32[]{:S(2)}) copy-start(u32[128]{0:T(128)} %constant.62) | copy-start | bytes 1540
  57.3 16.8 %copy-start.9 = (u32[128]{0:T(128)S(1)}, u32[128]{0:T(128)}, u32[]{:S(2)}) copy-start(u32[128]{0:T(128)} %constant.58) | copy-start | bytes 1540
Sparse Core Ops, SparseCore 0:
  73.6 19.8 all-gather.4
where the time goes:
time: 116 us
  waiting for transfers between devices  27.9 us (24%)
  blocking collectives  23.6 us (20%)
  starting transfers between devices  20.4 us (18%)
  local copies, waits for them, and re-layouts  15.6 us (13%)
  between operations  15.6 us (13%)
  matrix products  6.64 us (6%)
  other arithmetic  5.98 us (5%)
    all_gather x1, waiting for transfers between devices, total_of_pieces(): parts = lax.all_gather(array, axis).astype(jnp.float32)  15.5 us
    all_to_all x1, waiting for transfers between devices, shards(): lax.all_to_all(to_pieces(hidden_summary, sp_count, tp_count), SP_TP, spli...  12.3 us
    all_gather x1, blocking collectives, gather_together(): lines, at, finished = (lax.all_gather(line, axis), 0, [])  12.3 us
    all_to_all x1, starting transfers between devices, shards(): lax.all_to_all(to_pieces(rotary, sp_count, tp_count), SP_TP, split_axis=0...  11.5 us
    unnamed x2, blocking collectives  11.3 us
    unnamed x32, local copies, waits for them, and re-layouts  10.1 us
    all_to_all x1, starting transfers between devices, shards(): lax.all_to_all(to_pieces(hidden_summary, sp_count, tp_count), SP_TP, spli...  8.91 us
    dot_general x1, matrix products, shards(): jnp.dot(flat_rows, narrowing_matrix, preferred_element_type=jnp.float32)  2.9 us
  transfers between devices with their start and end apart: 3, of which 2 were waited for; matrix products, arithmetic and copies ran while one was open for 12% of the time, Pallas kernels for 0%

commit v1 on v0

--- a/solution.py
+++ b/solution.py
@@ -105,12 +105,18 @@
         jnp.bfloat16
     )
     moved = (
-        lax.all_to_all(
-            to_pieces(hidden_summary, sp_count, tp_count),
-            SP_TP,
-            split_axis=0,
-            concat_axis=2,
-            tiled=True,
+        jnp.concatenate(
+            lax.all_to_all(
+                jnp.stack(
+                    jnp.split(
+                        to_pieces(hidden_summary, sp_count, tp_count), lax.axis_size(SP_TP), axis=0
+                    )
+                ),
+                SP_TP,
+                0,
+                0,
+            ),
+            axis=2,
         ),
         lax.all_to_all(
             to_pieces(rotary, sp_count, tp_count), SP_TP, split_axis=0, concat_axis=2, tiled=True

time: 116 us -> 115 us (level)
  local copies, waits for them, and re-layouts: 15.6 us -> 14.1 us
    unnamed x32 -> x157, local copies, waits for them, and re-layouts: 10.1 us -> 9.53 us
where the time goes in v1:
time: 115 us
  waiting for transfers between devices  26.9 us (23%)
  blocking collectives  23.6 us (21%)
  starting transfers between devices  20.4 us (18%)
  between operations  16 us (14%)
  local copies, waits for them, and re-layouts  14.1 us (12%)
  matrix products  7.59 us (7%)
  other arithmetic  5.98 us (5%)
    all_gather x1, waiting for transfers between devices, total_of_pieces(): parts = lax.all_gather(array, axis).astype(jnp.float32)  15.5 us
    all_gather x1, blocking collectives, gather_together(): lines, at, finished = (lax.all_gather(line, axis), 0, [])  12.3 us
    all_to_all x1, starting transfers between devices, shards(): lax.all_to_all(to_pieces(rotary, sp_count, tp_count), SP_TP, split_axis=0...  11.5 us
    all_to_all x1, waiting for transfers between devices, shards(): lax.all_to_all(jnp.stack(jnp.split(to_pieces(hidden_summary, sp_count, tp...  11.4 us
    unnamed x2, blocking collectives  11.3 us
    unnamed x157, local copies, waits for them, and re-layouts  9.53 us
    all_to_all x1, starting transfers between devices, shards(): lax.all_to_all(jnp.stack(jnp.split(to_pieces(hidden_summary, sp_count, tp...  8.91 us
    dot_general x1, matrix products, shards(): jnp.dot(flat_rows, narrowing_matrix, preferred_element_type=jnp.float32)  2.9 us
  transfers between devices with their start and end apart: 3, of which 2 were waited for; matrix products, arithmetic and copies ran while one was open for 12% of the time, Pallas kernels for 0%

profile of v1, /device:TPU:1, one launch (start us, length us, event | category | flops | bytes accessed | tf_op | source)
XLA Modules:
  0.0 114.6 jit_solution(15294480907791573287)
XLA Ops:
  7.2 2.2 %fusion.2 = f32[16,32]{1,0:T(8,128)S(1)} fusion(bf16[16,32,2048]{2,1,0:T(8,128)(2,1)} %param.9), kind=kLoop, calls=%fused_computation.5 | loop fusion | flops 3145216 | bytes 2099200 | tf_op jit(solution)/shard_map/reduce_sum | solution.py:44
  9.6 0.5 fusion.4
  10.1 1.3 %copy-done.2 = bf16[16,32,2048]{2,1,0:T(8,128)(2,1)} copy-done((bf16[16,32,2048]{2,1,0:T(8,128)(2,1)}, bf16[16,32,2048]{2,1,0:T(8,128)(2,1)S(1)}, u32[]{:S(2)}) %copy-start.2) | copy-done | bytes 2097176
  11.5 0.8 fusion.5
  12.8 0.2 copy.669
  13.0 0.8 reshape.404
  13.8 11.5 %all-to-all-start.1 = ((bf16[128,2,128]{2,1,0:T(2,128)(2,1)}), bf16[128,2,128]{2,1,0:T(2,128)(2,1)S(1)}, u32[]{:S(2)}, u32[]{:S(2)}) async-start(bf16[128,2,128]{2,1,0:T(2,128)(2,1)} %reshape.404), calls=%async_computation.1 | async-start | bytes 131072 | tf_op jit(solution)/shard_map/all_to_all | solution.py:121
  25.4 12.3 %all-gather.2 = bf16[8,1,384]{2,1,0:T(2,128)(2,1)S(1)} all-gather(bf16[1,1,384]{2,1,0:T(2,128)(2,1)S(1)} %reshape.386), channel_id=2, replica_groups=mesh['sp'=16,'tp_0'=4,'tp_1'=2] {'tp_0','tp_1'}, dimensions={0}, use_global_device_ids=true | all-gather | bytes 6912 | tf_op jit(solution)/shard_map/all_gather | solution.py:23
  37.7 2.9 %fusion.7 = (f32[512]{0:T(512)S(1)}, bf16[512,512]{0,1:T(8,128)(2,1)S(1)}) fusion(bf16[512,2048]{1,0:T(8,128)(2,1)} %bitcast.713, bf16[2048,512]{1,0:T(8,128)(2,1)S(1)} %copy-done), kind=kOutput, calls=%fused_computation.16 | convolution fusion | flops 1074789888 | bytes 4720640 | tf_op jit(solution)/shard_map/dot_general | solution.py:90
  40.7 1.0 copy.540
  41.8 1.6 %reshape_reshape.3 = bf16[16,1,32,8,64]{4,3,2,0,1:T(8,128)(2,1)S(1)} reshape(bf16[512,512]{1,0:T(8,128)(2,1)} %copy.540) | data formatting | bytes 1048576 | tf_op jit(solution)/shard_map/reshape;reshape | solution.py:68
  43.4 0.2 copy.541
  45.3 1.4 %reshape.402 = bf16[128,2,1024]{2,1,0:T(2,128)(2,1)} reshape(bf16[128,1,1,32,64]{4,3,2,1,0:T(8,128)(2,1)S(1)} %constant_dynamic-update-slice_fusion) | data formatting | bytes 1048576
  46.7 8.9 %all-to-all-start = ((bf16[128,2,1024]{2,1,0:T(2,128)(2,1)}), bf16[128,2,1024]{2,1,0:T(2,128)(2,1)}, u32[]{:S(2)}, u32[]{:S(2)}) async-start(bf16[128,2,1024]{2,1,0:T(2,128)(2,1)} %reshape.402), calls=%async_computation | async-start | bytes 1048576 | tf_op jit(solution)/shard_map/all_to_all | solution.py:109
  55.8 1.2 %fusion.15 = f32[16,1,64]{2,1,0:T(1,128)S(1)} fusion(bf16[16,128,1]{1,2,0:T(2,128)(2,1)S(1)} %reshape.394, bf16[64,16,128]{2,1,0:T(8,128)(2,1)} %param.14), kind=kOutput, calls=%fused_computation.153 | convolution fusion | flops 262144 | bytes 270336 | tf_op jit(solution)/shard_map/shd,chd->shc/dot_general | solution.py:131
  57.2 0.3 reshape.378
  57.5 11.4 %all-to-all-done = bf16[128,2,1024]{2,1,0:T(2,128)(2,1)} async-done(((bf16[128,2,1024]{2,1,0:T(2,128)(2,1)}), bf16[128,2,1024]{2,1,0:T(2,128)(2,1)}, u32[]{:S(2)}, u32[]{:S(2)}) %all-to-all-start) | async-done | bytes 524320 | tf_op jit(solution)/shard_map/all_to_all | solution.py:109
  68.9 2.3 %reshape.403 = bf16[128,1,1,32,64]{4,3,2,1,0:T(8,128)(2,1)S(1)} reshape(bf16[128,2,1024]{2,1,0:T(2,128)(2,1)} %all-to-all-done) | data formatting | bytes 1048576
  71.1 0.4 fusion.26
  71.5 0.9 fusion.1
  72.4 0.6 dynamic-slice.2
  73.0 0.6 dynamic-slice
  74.9 0.9 squeeze.3
  75.8 1.1 copy.674
  76.9 15.5 %all-gather.5.cloned.1.call-done = bf16[128,4096]{1,0:T(8,128)(2,1)} async-done(((bf16[16,4096]{1,0:T(8,128)(2,1)}), bf16[128,4096]{1,0:T(8,128)(2,1)}) %all-gather.5.cloned.1.call-update) | async-done | bytes 1048592 | tf_op jit(solution)/shard_map/all_gather | solution.py:32
  92.5 1.4 %convert_reduce_fusion = f32[16,4096]{1,0:T(8,128)S(1)} fusion(bf16[8,16,4096]{2,1,0:T(8,128)(2,1)} %bitcast.844), kind=kLoop, calls=%fused_computation.8 | loop fusion | flops 983040 | bytes 1310720 | tf_op jit(solution)/shard_map/reduce_sum | solution.py:33
  94.0 0.2 exponential_reduce_fusion
  94.3 0.3 fusion.6
  94.6 1.1 %fusion.13 = f32[16,1,128]{2,1,0:T(1,128)S(1)} fusion(bf16[64,16,128]{2,1,0:T(8,128)(2,1)} %param.15, bf16[16,64,1]{1,0,2:T(8,128)(2,1)S(1)} %fusion.6), kind=kOutput, calls=%fused_computation.151 | convolution fusion | flops 262144 | bytes 272384 | tf_op jit(solution)/shard_map/shc,chv->hsv/dot_general | solution.py:150
  95.7 6.9 %all-reduce = f32[16,1,128]{2,0,1:T(8,128)S(1)} all-reduce(f32[16,1,128]{2,0,1:T(8,128)S(1)} %bitcast.850), channel_id=4, replica_groups=mesh['sp'=16,'tp_0'=4,'tp_1'=2] {'tp_0'}, use_global_device_ids=true, to_apply=%region_5.0.clone | all-reduce | flops 2048 | bytes 16384
  102.6 4.4 %all-reduce.1 = f32[4,1,128]{2,0,1:T(4,128)S(1)} all-reduce(f32[4,1,128]{2,0,1:T(4,128)S(1)} %constant_dynamic-slice_fusion), channel_id=5, replica_groups=mesh['sp'=16,'tp_0'=4,'tp_1'=2] {'tp_1'}, use_global_device_ids=true, to_apply=%region_6.0.clone | all-reduce | flops 512 | bytes 4096
  107.2 0.6 multiply_convert_fusion
  (175 shorter events, 2.9 us)
Async XLA Ops:
  7.2 30.5 %copy-start = (bf16[2048,512]{1,0:T(8,128)(2,1)S(1)}, bf16[2048,512]{1,0:T(8,128)(2,1)}, u32[]{:S(2)}) copy-start(bf16[2048,512]{1,0:T(8,128)(2,1)} %param.11) | copy-start | bytes 6291460
  7.2 2.3 %copy-start.4 = (f32[2048]{0:T(1024)S(1)}, f32[2048]{0:T(1024)}, u32[]{:S(2)}) copy-start(f32[2048]{0:T(1024)} %param.10) | copy-start | bytes 24580
  7.2 2.3 %copy-start.1 = (bf16[16,32,2048]{2,1,0:T(8,128)(2,1)S(1)}, bf16[16,32,2048]{2,1,0:T(8,128)(2,1)}, u32[]{:S(2)}) copy-start(bf16[16,32,2048]{2,1,0:T(8,128)(2,1)} %param.9) | copy-start | bytes 6291460
  9.6 1.9 %copy-start.3 = (bf16[2048,64]{0,1:T(8,128)(2,1)S(1)}, bf16[2048,64]{0,1:T(8,128)(2,1)}, u32[]{:S(2)}) copy-start(bf16[2048,64]{0,1:T(8,128)(2,1)} %param.12) | copy-start | bytes 786436
  10.1 1.4 %copy-start.2 = (bf16[16,32,2048]{2,1,0:T(8,128)(2,1)}, bf16[16,32,2048]{2,1,0:T(8,128)(2,1)S(1)}, u32[]{:S(2)}) copy-start(bf16[16,32,2048]{2,1,0:T(8,128)(2,1)S(1)} %fusion.4) | copy-start | bytes 6291460
  11.5 13.8 %copy-start.7 = (bf16[1,2,64]{2,1,0:T(2,128)(2,1)S(1)}, bf16[1,2,64]{2,1,0:T(2,128)(2,1)}, u32[]{:S(2)}) copy-start(bf16[1,2,64]{2,1,0:T(2,128)(2,1)} %param.17) | copy-start | bytes 772
  11.5 13.9 %copy-start.6 = (bf16[1,2,128]{2,1,0:T(2,128)(2,1)S(1)}, bf16[1,2,128]{2,1,0:T(2,128)(2,1)}, u32[]{:S(2)}) copy-start(bf16[1,2,128]{2,1,0:T(2,128)(2,1)} %param.16) | copy-start | bytes 1540
  13.8 32.9 %all-to-all-start.1 = ((bf16[128,2,128]{2,1,0:T(2,128)(2,1)}), bf16[128,2,128]{2,1,0:T(2,128)(2,1)S(1)}, u32[]{:S(2)}, u32[]{:S(2)}) async-start(bf16[128,2,128]{2,1,0:T(2,128)(2,1)} %reshape.404), calls=%async_computation.1 | async-start | bytes 131072 | tf_op jit(solution)/shard_map/all_to_all | solution.py:121
  37.7 2.9 %copy-start.5 = (f32[512]{0:T(512)S(1)}, f32[512]{0:T(512)}, u32[]{:S(2)}) copy-start(f32[512]{0:T(512)} %param.13) | copy-start | bytes 6148
  46.7 22.2 %all-to-all-start = ((bf16[128,2,1024]{2,1,0:T(2,128)(2,1)}), bf16[128,2,1024]{2,1,0:T(2,128)(2,1)}, u32[]{:S(2)}, u32[]{:S(2)}) async-start(bf16[128,2,1024]{2,1,0:T(2,128)(2,1)} %reshape.402), calls=%async_computation | async-start | bytes 1048576 | tf_op jit(solution)/shard_map/all_to_all | solution.py:109
  55.6 36.9 %all-gather.5.cloned.1.call-start = ((), (), s32[]{:S(2)}) async-start(), calls=%async_computation.2 | async-start | bytes 1179648 | tf_op jit(solution)/shard_map/all_gather | solution.py:32
  57.2 15.3 %copy-start.9 = (u32[128]{0:T(128)S(1)}, u32[128]{0:T(128)}, u32[]{:S(2)}) copy-start(u32[128]{0:T(128)} %constant.62) | copy-start | bytes 1540
  57.2 15.9 %copy-start.8 = (u32[128]{0:T(128)S(1)}, u32[128]{0:T(128)}, u32[]{:S(2)}) copy-start(u32[128]{0:T(128)} %constant.58) | copy-start | bytes 1540
Sparse Core Ops, SparseCore 0:
  72.5 19.8 all-gather.4
